TPU v7x, 128 devices: a whole 4x4x4 slice. The times are simulated.
128 devices in a mesh: rep: 2 (over z_hi), fs: 32 (over z_lo, y, x), tp: 2 (over core).
Axes of the slice: x: 4, y: 4, z: 4 (z_hi: 2, z_lo: 2; z = z_hi * 2 + z_lo), core: 2. Of those that a mesh axis runs over, the one named last changes fastest.
Arguments:
- tokens: bfloat16 [65536, 2048], P(('rep', 'fs')), may hold values from -6 to 6
- norm_mix: bfloat16 [2048], replicated, may hold values from 0.099609375 to 1.8984375
- w_unit: bfloat16 [2048, 1024], P('fs', 'tp'), may hold values from -0.125 to 0.125
- w_value: bfloat16 [2048, 1024], P('fs', 'tp'), may hold values from -0.125 to 0.125
- spatial: bfloat16 [4, 128, 128], replicated, may hold values from -0.52734375 to 0.52734375
- spatial_bias: bfloat16 [4, 128], replicated, may hold values from 0.099609375 to 1.8984375
- group_gain: bfloat16 [1024], replicated, may hold values from 0.099609375 to 1.8984375
- group_shift: bfloat16 [1024], replicated, may hold values from -3 to 3
- w_mix_out: bfloat16 [1024, 2048], P('tp', 'fs'), may hold values from -0.1875 to 0.1875
- norm_ffn: bfloat16 [2048], replicated, may hold values from 0.099609375 to 1.8984375
- w_gate: bfloat16 [2048, 2816], P('fs', 'tp'), may hold values from -0.125 to 0.125
- w_up: bfloat16 [2048, 2816], P('fs', 'tp'), may hold values from -0.125 to 0.125
- w_down: bfloat16 [2816, 2048], P('tp', 'fs'), may hold values from -0.109375 to 0.109375
Outputs:
- layer_out: bfloat16 [65536, 2048], P(('rep', 'fs', 'tp'))
All inputs are finite; a program needn't handle non-finite values.
Results may differ from a plain program's by a relative error of at most 0.008.
Values may be sent and summed in bfloat16 or wider, within the bound.
No kernel may reach another device: no remote copies, remote signals or barrier semaphores. Data moves between devices by JAX's collectives and lax.ppermute only.
A program may use at most 128 MiB of HBM per device.

v0:
```python
import jax
import jax.numpy as jnp
from jax import lax
from jax.sharding import PartitionSpec as P


def sent_together(arrays, axis, dim, along):
    ends, at = ([], 0)
    for a in arrays[:-1]:
        at += a.shape[along]
        ends.append(at)
    both = jnp.concatenate(arrays, axis=along)
    return tuple(jnp.split(lax.all_gather(both, axis, axis=dim, tiled=True), ends, axis=along))


def sent_to_all(x, axis):
    copies = jnp.broadcast_to(x, (lax.axis_size(axis), *x.shape))
    return lax.all_to_all(copies, axis, split_axis=0, concat_axis=0, tiled=True)


def in_order(pieces, dim):
    pieces = jnp.moveaxis(pieces, 0, dim)
    dims = pieces.shape
    return pieces.reshape(*dims[:dim], dims[dim] * dims[dim + 1], *dims[dim + 2 :])


def gathered_copies(x, axis, dim):
    pieces = sent_to_all(x, axis)
    return in_order(pieces, dim)


def total_of_pieces(x, axis):
    return lax.all_gather(x, axis).sum(0)


def split_up(x, dim, peers):
    before, after = (x.shape[:dim], x.shape[dim + 1 :])
    return jnp.moveaxis(x.reshape(*before, peers, -1, *after), dim, 0)


def summed_on_arrival(x, axis, dim):
    pieces = split_up(x, dim, lax.axis_size(axis))
    arrived = lax.all_to_all(pieces, axis, split_axis=0, concat_axis=0, tiled=True)
    return arrived.astype(jnp.float32).sum(axis=0)


def rms_scale(values, gain):
    values = values.astype(jnp.float32)
    scale = lax.rsqrt(jnp.mean(values * values, axis=-1, keepdims=True) + 1e-06)
    return values * scale * gain.astype(jnp.float32)


def spatial_unit(unit_pre, value_pre, spatial, spatial_bias, group_gain, group_shift):
    count, width = value_pre.shape
    groups = spatial.shape[0]
    block = spatial.shape[1]
    active = jax.nn.gelu(value_pre, approximate=True).reshape(count, groups, width // groups)
    center = jnp.mean(active, axis=-1, keepdims=True)
    spread = jnp.mean(jnp.square(active - center), axis=-1, keepdims=True)
    normal = ((active - center) * lax.rsqrt(spread + 1e-06)).reshape(count, width)
    normal = normal * group_gain.astype(jnp.float32) + group_shift.astype(jnp.float32)
    grouped = normal.astype(jnp.bfloat16)
    causal = jnp.tril(jnp.ones((block, block), dtype=bool))
    weights = jnp.where(causal[None], spatial, jnp.zeros_like(spatial))
    tiles = grouped.reshape(count // block, block, groups, width // groups)
    mixed = jnp.einsum("gts,nsgd->ntgd", weights, tiles, preferred_element_type=jnp.float32)
    mixed = mixed + spatial_bias.astype(jnp.float32).T[None, :, :, None]
    return jax.nn.gelu(unit_pre, approximate=True) * mixed.reshape(count, width)


def on_device(
    tokens,
    norm_mix,
    w_unit,
    w_value,
    spatial,
    spatial_bias,
    group_gain,
    group_shift,
    w_mix_out,
    norm_ffn,
    w_gate,
    w_up,
    w_down,
):
    count = tokens.shape[0]
    half = count // lax.axis_size("tp")
    position = lax.axis_index("tp")
    row_start = position * half
    local_width = w_unit.shape[1]
    group_count = spatial.shape[0] // lax.axis_size("tp")
    group_start = position * group_count
    spatial_local = lax.dynamic_slice_in_dim(spatial, group_start, group_count, 0)
    bias_local = lax.dynamic_slice_in_dim(spatial_bias, group_start, group_count, 0)
    gain_local = lax.dynamic_slice_in_dim(group_gain, position * local_width, local_width, 0)
    shift_local = lax.dynamic_slice_in_dim(group_shift, position * local_width, local_width, 0)
    normed = rms_scale(tokens, norm_mix).astype(jnp.bfloat16)
    unit_whole, value_whole = sent_together((w_unit, w_value), "fs", 0, 1)
    unit_pre = jnp.dot(normed, unit_whole, preferred_element_type=jnp.float32)
    value_pre = jnp.dot(normed, value_whole, preferred_element_type=jnp.float32)
    gated = spatial_unit(
        unit_pre, value_pre, spatial_local, bias_local, gain_local, shift_local
    ).astype(jnp.bfloat16)
    partial_terms = jnp.dot(
        gated, gathered_copies(w_mix_out, "fs", 1), preferred_element_type=jnp.float32
    )
    summed = total_of_pieces(partial_terms, "tp")
    h_mid = (tokens.astype(jnp.float32) + summed).astype(jnp.bfloat16)
    normed_mid = rms_scale(h_mid, norm_ffn).astype(jnp.bfloat16)
    gate_whole, up_whole = sent_together((w_gate, w_up), "fs", 0, 1)
    gate = jnp.dot(normed_mid, gate_whole, preferred_element_type=jnp.float32)
    up = jnp.dot(normed_mid, up_whole, preferred_element_type=jnp.float32)
    hidden = (jax.nn.silu(gate) * up).astype(jnp.bfloat16)
    down_cols = lax.all_gather(w_down, "fs", axis=1, tiled=True)
    residual_rows = lax.dynamic_slice_in_dim(h_mid, row_start, half, 0).astype(jnp.float32)
    summed_rows = summed_on_arrival(
        jnp.dot(hidden, down_cols, preferred_element_type=jnp.float32).astype(jnp.bfloat16), "tp", 0
    )
    return (residual_rows + summed_rows).astype(jnp.bfloat16)


def solution(mesh):
    placed = (
        P(("rep", "fs"), None),
        P(),
        P("fs", "tp"),
        P("fs", "tp"),
        P(),
        P(),
        P(),
        P(),
        P("tp", "fs"),
        P(),
        P("fs", "tp"),
        P("fs", "tp"),
        P("tp", "fs"),
    )
    return jax.shard_map(
        on_device,
        mesh=mesh,
        in_specs=placed,
        out_specs=P(("rep", "fs", "tp"), None),
        check_vma=False,
    )
```

profile of v0, /device:TPU:1, one launch (start us, length us, event | category | flops | bytes accessed | tf_op | source)
XLA Modules:
  0.0 629.2 jit_solution(16438548954573870074)
XLA Ops:
  6.6 1.6 pad_maximum_fusion.1
  8.2 2.4 broadcast_in_dim.13
  10.6 9.3 %all-to-all-start = ((bf16[32,512,64]{1,2,0:T(8,128)(2,1)}), bf16[32,512,64]{1,2,0:T(8,128)(2,1)}, u32[]{:S(2)}, u32[]{:S(2)}) async-start(bf16[32,512,64]{1,2,0:T(8,128)(2,1)} %broadcast_in_dim.13), calls=%async_computation | async-start | bytes 4194304 | tf_op jit(solution)/shard_map/all_to_all | solution.py:18
  20.1 3.1 fusion.3
  23.3 133.9 %all-gather.6.cloned.1.call-done = bf16[2048,1024]{1,0:T(8,128)(2,1)} async-done(((bf16[64,1024]{1,0:T(8,128)(2,1)}), bf16[2048,1024]{1,0:T(8,128)(2,1)}) %all-gather.6.cloned.1.call-update) | async-done | bytes 4194320 | tf_op jit(solution)/shard_map/all_gather | solution.py:13
  157.1 6.9 %fusion.35 = f32[1024,512]{1,0:T(8,128)} fusion(bf16[2048,1024]{1,0:T(8,128)(2,1)} %all-gather.6.cloned.1.call-done, bf16[1024,2048]{1,0:T(8,128)(2,1)} %param.13, f32[2048]{0:T(1024)S(1)} %convert_element_type.51, f32[1024]{0:T(1024)S(1)} %add_rsqrt_fusion.2), kind=kOutput, calls=%fused_computation.39 | convolution fusion | flops 2160066560 | bytes 8400896 | tf_op jit(solution)/shard_map/dot_general | solution.py:100
  164.1 2.6 reshape.58
  166.7 1.2 reduce_sum.55
  167.9 14.4 %multiply_reduce_fusion = f32[1024,2]{1,0:T(8,128)S(1)} fusion(f32[1024,2,256]{2,1,0:T(2,128)S(1)} %reshape.58, f32[1024,2]{1,0:T(8,128)S(1)} %broadcast_multiply_fusion), kind=kLoop, calls=%fused_computation.46 | loop fusion | flops 1570816 | bytes 2113536 | tf_op jit(solution)/shard_map/reduce_sum | solution.py:59
  182.4 1.2 mul.112
  183.8 1.2 sub.17
  187.1 2.4 copy.28
  189.5 1.8 copy.33
  191.3 11.6 %fusion.51 = f32[1024,2048]{1,0:T(8,128)} fusion(bf16[512,2048]{0,1:T(8,128)(2,1)} %bitcast.5, f32[1024,512]{1,0:T(8,128)S(1)} %bitcast.30, bf16[2048,1024]{1,0:T(8,128)(2,1)} %all-gather.6.cloned.1.call-done, bf16[1024,2048]{1,0:T(8,128)(2,1)} %param.13, f32[2048]{0:T(1024)S(1)} %convert_element_type.51, f32[1024]{0:T(1024)S(1)} %add_rsqrt_fusion.2), kind=kOutput, calls=%fused_computation.47 | convolution fusion | flops 4308598784 | bytes 18886656 | tf_op jit(solution)/shard_map/dot_general | solution.py:104
  205.3 49.1 %all-gather.12.cloned.1.call-done = f32[2048,2048]{1,0:T(8,128)} async-done(((f32[1024,2048]{1,0:T(8,128)}), f32[2048,2048]{1,0:T(8,128)}) %all-gather.12.cloned.1.call-update) | async-done | bytes 16777232 | tf_op jit(solution)/shard_map/all_gather | solution.py:33
  254.4 11.8 %reduce_sum.57 = f32[1024,2048]{1,0:T(8,128)} reduce(f32[2,1024,2048]{2,1,0:T(8,128)} %bitcast.23, f32[]{:T(128)} %constant.15.clone.1), dimensions={0}, to_apply=%region_3.4 | reduce | flops 2097152 | bytes 25165828 | tf_op jit(solution)/shard_map/reduce_sum | solution.py:33
  266.1 7.8 %fusion = (f32[1024]{0:T(1024)S(1)}, bf16[1024,2048]{1,0:T(8,128)(2,1)}) fusion(f32[1024,2048]{1,0:T(8,128)} %reduce_sum.57, bf16[1024,2048]{1,0:T(8,128)(2,1)} %param.13), kind=kLoop, calls=%fused_computation.5 | loop fusion | flops 12581888 | bytes 16781312 | tf_op jit(solution)/shard_map/reduce_sum | solution.py:49
  273.9 135.7 %all-gather.8.cloned.1.call-done = bf16[2048,2816]{1,0:T(8,128)(2,1)} async-done(((bf16[64,2816]{1,0:T(8,128)(2,1)}), bf16[2048,2816]{1,0:T(8,128)(2,1)}) %all-gather.8.cloned.1.call-update) | async-done | bytes 11534352 | tf_op jit(solution)/shard_map/all_gather | solution.py:13
  409.6 11.9 %fusion.9 = f32[1024,1408]{1,0:T(8,128)} fusion(bf16[2048,2816]{1,0:T(8,128)(2,1)} %all-gather.8.cloned.1.call-done, bf16[1024,2048]{1,0:T(8,128)(2,1)} %get-tuple-element.6, f32[2048]{0:T(1024)S(1)} %convert_element_type.60, f32[1024]{0:T(1024)S(1)} %add_rsqrt_fusion.1), kind=kOutput, calls=%fused_computation.15 | convolution fusion | flops 5913968640 | bytes 15740928 | tf_op jit(solution)/shard_map/dot_general | solution.py:111
  421.5 147.9 %all-gather.10.cloned.1.call-done = bf16[1408,2048]{0,1:T(8,128)(2,1)} async-done(((bf16[1408,64]{0,1:T(8,128)(2,1)}), bf16[1408,2048]{0,1:T(8,128)(2,1)}) %all-gather.10.cloned.1.call-update) | async-done | bytes 5767184 | tf_op jit(solution)/shard_map/all_gather | solution.py:114
  569.4 20.9 %fusion.16 = bf16[1024,2048]{1,0:T(8,128)(2,1)} fusion(bf16[1408,2048]{0,1:T(8,128)(2,1)} %all-gather.10.cloned.1.call-done, f32[1024,1408]{1,0:T(8,128)} %fusion.9, bf16[2048,2816]{1,0:T(8,128)(2,1)} %all-gather.8.cloned.1.call-done, bf16[1024,2048]{1,0:T(8,128)(2,1)} %get-tuple-element.6, f32[2048]{0:T(1024)S(1)} %convert_element_type.60, ...), kind=kOutput, calls=%fused_computation.20 | convolution fusion | flops 11830296576 | bytes 25702400 | tf_op jit(solution)/shard_map/dot_general | solution.py:117
  590.3 28.2 %all_to_all.10 = bf16[2,512,2048]{2,1,0:T(8,128)(2,1)S(1)} all-to-all(bf16[2,512,2048]{2,1,0:T(8,128)(2,1)} %bitcast.29), channel_id=1, replica_groups=mesh['rep'=2,'fs'=32,'tp'=2] {'tp'}, dimensions={0} | all-to-all | bytes 8388608 | tf_op jit(solution)/shard_map/all_to_all | solution.py:43
  619.4 1.2 copy-done
  620.7 2.1 add_convert_fusion
  (44 shorter events, 5.8 us)
Async XLA Ops:
  6.5 13.4 %copy-start.5 = (bf16[2048]{0:T(1024)(128)(2,1)S(1)}, bf16[2048]{0:T(1024)(128)(2,1)}, u32[]{:S(2)}) copy-start(bf16[2048]{0:T(1024)(128)(2,1)} %param.14) | copy-start | bytes 12292
  6.5 13.5 %copy-start.9 = (bf16[4,128]{1,0:T(4,128)(2,1)S(1)}, bf16[4,128]{1,0:T(4,128)(2,1)}, u32[]{:S(2)}) copy-start(bf16[4,128]{1,0:T(4,128)(2,1)} %param.18) | copy-start | bytes 3076
  6.5 13.5 %copy-start.8 = (bf16[1024]{0:T(1024)(128)(2,1)S(1)}, bf16[1024]{0:T(1024)(128)(2,1)}, u32[]{:S(2)}) copy-start(bf16[1024]{0:T(1024)(128)(2,1)} %param.19) | copy-start | bytes 6148
  6.5 13.5 %copy-start.7 = (bf16[1024]{0:T(1024)(128)(2,1)S(1)}, bf16[1024]{0:T(1024)(128)(2,1)}, u32[]{:S(2)}) copy-start(bf16[1024]{0:T(1024)(128)(2,1)} %param.20) | copy-start | bytes 6148
  6.5 150.6 %all-gather.6.cloned.1.call-start = ((), (), s32[]{:S(2)}) async-start(), calls=%async_computation.2 | async-start | bytes 4325376 | tf_op jit(solution)/shard_map/all_gather | solution.py:13
  10.6 180.7 %all-to-all-start = ((bf16[32,512,64]{1,2,0:T(8,128)(2,1)}), bf16[32,512,64]{1,2,0:T(8,128)(2,1)}, u32[]{:S(2)}, u32[]{:S(2)}) async-start(bf16[32,512,64]{1,2,0:T(8,128)(2,1)} %broadcast_in_dim.13), calls=%async_computation | async-start | bytes 4194304 | tf_op jit(solution)/shard_map/all_to_all | solution.py:18
  19.9 234.4 %all-gather.12.cloned.1.call-start = ((), (), s32[]{:S(2)}) async-start(), calls=%async_computation.5 | async-start | bytes 25165824 | tf_op jit(solution)/shard_map/all_gather | solution.py:33
  183.8 1.6 copy-start.1
  185.4 1.1 copy-start.4
  202.9 0.9 copy-start.2
  202.9 1.0 copy-start.3
  202.9 2.4 copy-start.6
  202.9 206.7 %all-gather.8.cloned.1.call-start = ((), (), s32[]{:S(2)}) async-start(), calls=%async_computation.3 | async-start | bytes 11894784 | tf_op jit(solution)/shard_map/all_gather | solution.py:13
  204.7 364.7 %all-gather.10.cloned.1.call-start = ((), (), s32[]{:S(2)}) async-start(), calls=%async_computation.4 | async-start | bytes 5947392 | tf_op jit(solution)/shard_map/all_gather | solution.py:114
  618.5 2.2 copy-start
Sparse Core Ops, SparseCore 0:
  9.0 148.1 all-gather.5
  203.0 51.2 all-gather.11
  256.0 153.5 all-gather.7
  411.1 158.2 all-gather.9
where the time goes:
time: 630 us; the launch traced here: 629 us
  waiting for transfers between devices  467 us (74%)
  matrix products  51.8 us (8%)
  other arithmetic  44.6 us (7%)
  blocking collectives  28.2 us (4%)
  local copies, waits for them, and re-layouts  14.5 us (2%)
  between operations  13.3 us (2%)
  starting transfers between devices  9.5 us (2%)
    all_gather x2, waiting for transfers between devices, sent_together(): lax.all_gather(both, axis, axis=dim, tiled=True)  270 us
    all_gather x1, waiting for transfers between devices, on_device(): down_cols = lax.all_gather(w_down, 'fs', axis=1, tiled=True)  148 us
    all_gather x1, waiting for transfers between devices, total_of_pieces(): return lax.all_gather(x, axis).sum(0)  49.1 us
    all_to_all x1, blocking collectives, summed_on_arrival(): lax.all_to_all(pieces, axis, split_axis=0, concat_axis=0, tiled=True)  28.2 us
    dot_general x1, matrix products, on_device(): jnp.dot(hidden, down_cols, preferred_element_type=jnp.float32)  20.9 us
    reduce_sum x1, other arithmetic, spatial_unit(): spread = jnp.mean(jnp.square(active - center), axis=-1, keepdims=True)  14.4 us
  transfers between devices with their start and end apart: 5, of which 4 were waited for; matrix products, arithmetic and copies ran while one was open for 11% of the time, Pallas kernels for 0%

commit v1 on v0

--- a/solution.py
+++ b/solution.py
@@ -111,7 +111,7 @@
     gate = jnp.dot(normed_mid, gate_whole, preferred_element_type=jnp.float32)
     up = jnp.dot(normed_mid, up_whole, preferred_element_type=jnp.float32)
     hidden = (jax.nn.silu(gate) * up).astype(jnp.bfloat16)
-    down_cols = lax.all_gather(w_down, "fs", axis=1, tiled=True)
+    down_cols = jnp.concatenate(lax.all_gather(w_down, "fs"), axis=1)
     residual_rows = lax.dynamic_slice_in_dim(h_mid, row_start, half, 0).astype(jnp.float32)
     summed_rows = summed_on_arrival(
         jnp.dot(hidden, down_cols, preferred_element_type=jnp.float32).astype(jnp.bfloat16), "tp", 0

time: 630 us -> 600 us (0.952)
  waiting for transfers between devices: 467 us -> 429 us
  local copies, waits for them, and re-layouts: 14.5 us -> 22.5 us
    all_gather x1, waiting for transfers between devices: 148 us -> 113 us  [on_device(): down_cols = jnp.concatenate(lax.all_gather(w_down, 'fs'), axis=1)]
  transfers between devices with their start and end apart: 5 -> 5, of which waited for: 4 -> 4; matrix products, arithmetic and copies ran while one was open for 11% -> 13% of each run, Pallas kernels for 0% -> 0%
where the time goes in v1:
time: 600 us
  waiting for transfers between devices  429 us (72%)
  matrix products  51.9 us (9%)
  other arithmetic  44.6 us (7%)
  blocking collectives  28.2 us (5%)
  local copies, waits for them, and re-layouts  22.5 us (4%)
  between operations  13.4 us (2%)
  starting transfers between devices  9.5 us (2%)
    all_gather x2, waiting for transfers between devices, sent_together(): lax.all_gather(both, axis, axis=dim, tiled=True)  269 us
    all_gather x1, waiting for transfers between devices, on_device(): down_cols = jnp.concatenate(lax.all_gather(w_down, 'fs'), axis=1)  113 us
    all_gather x1, waiting for transfers between devices, total_of_pieces(): return lax.all_gather(x, axis).sum(0)  47 us
    all_to_all x1, blocking collectives, summed_on_arrival(): lax.all_to_all(pieces, axis, split_axis=0, concat_axis=0, tiled=True)  28.2 us
    dot_general x1, matrix products, on_device(): jnp.dot(hidden, down_cols, preferred_element_type=jnp.float32)  20.9 us
    reduce_sum x1, other arithmetic, spatial_unit(): spread = jnp.mean(jnp.square(active - center), axis=-1, keepdims=True)  14.4 us
  transfers between devices with their start and end apart: 5, of which 4 were waited for; matrix products, arithmetic and copies ran while one was open for 13% of the time, Pallas kernels for 0%

profile of v1, /device:TPU:1, one launch (start us, length us, event | category | flops | bytes accessed | tf_op | source)
XLA Modules:
  0.0 599.6 jit_solution(1685834223399084839)
XLA Ops:
  6.6 1.6 pad_maximum_fusion.1
  8.9 2.4 broadcast_in_dim.13
  11.3 9.3 %all-to-all-start = ((bf16[32,512,64]{1,2,0:T(8,128)(2,1)}), bf16[32,512,64]{1,2,0:T(8,128)(2,1)}, u32[]{:S(2)}, u32[]{:S(2)}) async-start(bf16[32,512,64]{1,2,0:T(8,128)(2,1)} %broadcast_in_dim.13), calls=%async_computation | async-start | bytes 4194304 | tf_op jit(solution)/shard_map/all_to_all | solution.py:18
  20.9 3.1 fusion.3
  24.0 133.0 %all-gather.7.cloned.1.call-done = bf16[2048,1024]{1,0:T(8,128)(2,1)} async-done(((bf16[64,1024]{1,0:T(8,128)(2,1)}), bf16[2048,1024]{1,0:T(8,128)(2,1)}) %all-gather.7.cloned.1.call-update) | async-done | bytes 4194320 | tf_op jit(solution)/shard_map/all_gather | solution.py:13
  157.0 6.9 %fusion.35 = f32[1024,512]{1,0:T(8,128)} fusion(bf16[2048,1024]{1,0:T(8,128)(2,1)} %all-gather.7.cloned.1.call-done, bf16[1024,2048]{1,0:T(8,128)(2,1)} %param.13, f32[2048]{0:T(1024)S(1)} %convert_element_type.51, f32[1024]{0:T(1024)S(1)} %add_rsqrt_fusion.2), kind=kOutput, calls=%fused_computation.39 | convolution fusion | flops 2160066560 | bytes 8400896 | tf_op jit(solution)/shard_map/dot_general | solution.py:100
  163.9 2.6 reshape.64
  167.7 14.4 %multiply_reduce_fusion = f32[1024,2]{1,0:T(8,128)S(1)} fusion(f32[1024,2,256]{2,1,0:T(2,128)S(1)} %reshape.64, f32[1024,2]{1,0:T(8,128)S(1)} %broadcast_multiply_fusion), kind=kLoop, calls=%fused_computation.46 | loop fusion | flops 1570816 | bytes 2113536 | tf_op jit(solution)/shard_map/reduce_sum | solution.py:59
  182.3 1.2 mul.112
  183.7 1.2 sub.17
  186.9 2.4 copy.35
  189.3 1.8 copy.41
  191.1 11.7 %fusion.51 = f32[1024,2048]{1,0:T(8,128)} fusion(bf16[512,2048]{0,1:T(8,128)(2,1)} %bitcast.5, f32[1024,512]{1,0:T(8,128)S(1)} %bitcast.40, bf16[2048,1024]{1,0:T(8,128)(2,1)} %all-gather.7.cloned.1.call-done, bf16[1024,2048]{1,0:T(8,128)(2,1)} %param.13, f32[2048]{0:T(1024)S(1)} %convert_element_type.51, f32[1024]{0:T(1024)S(1)} %add_rsqrt_fusion.2), kind=kOutput, calls=%fused_computation.47 | convolution fusion | flops 4308598784 | bytes 18886656 | tf_op jit(solution)/shard_map/dot_general | solution.py:104
  204.6 113.1 %all-gather.13.cloned.1.call-done = bf16[45056,64]{0,1:T(8,128)(2,1)} async-done(((bf16[1408,64]{0,1:T(8,128)(2,1)}), bf16[45056,64]{0,1:T(8,128)(2,1)}) %all-gather.13.cloned.1.call-update) | async-done | bytes 5767184 | tf_op jit(solution)/shard_map/all_gather | solution.py:114
  317.7 3.5 copy.42
  321.3 4.5 copy.36
  325.7 47.0 %all-gather.11.cloned.1.call-done = f32[2048,2048]{1,0:T(8,128)} async-done(((f32[1024,2048]{1,0:T(8,128)}), f32[2048,2048]{1,0:T(8,128)}) %all-gather.11.cloned.1.call-update) | async-done | bytes 16777232 | tf_op jit(solution)/shard_map/all_gather | solution.py:33
  372.8 11.8 %reduce_sum.57 = f32[1024,2048]{1,0:T(8,128)} reduce(f32[2,1024,2048]{2,1,0:T(8,128)} %bitcast.31, f32[]{:T(128)} %constant.15.clone.1), dimensions={0}, to_apply=%region_3.4 | reduce | flops 2097152 | bytes 25165828 | tf_op jit(solution)/shard_map/reduce_sum | solution.py:33
  384.5 7.8 %fusion = (f32[1024]{0:T(1024)S(1)}, bf16[1024,2048]{1,0:T(8,128)(2,1)}) fusion(f32[1024,2048]{1,0:T(8,128)} %reduce_sum.57, bf16[1024,2048]{1,0:T(8,128)(2,1)} %param.13), kind=kLoop, calls=%fused_computation.5 | loop fusion | flops 12581888 | bytes 16781312 | tf_op jit(solution)/shard_map/reduce_sum | solution.py:49
  392.3 135.6 %all-gather.9.cloned.1.call-done = bf16[2048,2816]{1,0:T(8,128)(2,1)} async-done(((bf16[64,2816]{1,0:T(8,128)(2,1)}), bf16[2048,2816]{1,0:T(8,128)(2,1)}) %all-gather.9.cloned.1.call-update) | async-done | bytes 11534352 | tf_op jit(solution)/shard_map/all_gather | solution.py:13
  527.8 11.9 %fusion.9 = f32[1024,1408]{1,0:T(8,128)} fusion(bf16[2048,2816]{1,0:T(8,128)(2,1)} %all-gather.9.cloned.1.call-done, bf16[1024,2048]{1,0:T(8,128)(2,1)} %get-tuple-element.6, f32[2048]{0:T(1024)S(1)} %convert_element_type.60, f32[1024]{0:T(1024)S(1)} %add_rsqrt_fusion.1), kind=kOutput, calls=%fused_computation.15 | convolution fusion | flops 5913968640 | bytes 15740928 | tf_op jit(solution)/shard_map/dot_general | solution.py:111
  539.7 20.9 %fusion.16 = bf16[1024,2048]{1,0:T(8,128)(2,1)} fusion(bf16[1408,2048]{0,1:T(8,128)(2,1)} %bitcast.38, f32[1024,1408]{1,0:T(8,128)} %fusion.9, bf16[2048,2816]{1,0:T(8,128)(2,1)} %all-gather.9.cloned.1.call-done, bf16[1024,2048]{1,0:T(8,128)(2,1)} %get-tuple-element.6, f32[2048]{0:T(1024)S(1)} %convert_element_type.60, f32[1024]{0:T(1024)S(1)} %add_rsqrt_fusion.1), kind=kOutput, calls=%fused_computation.20 | convolution fusion | flops 11830296576 | bytes 25702400 | tf_op jit(solution)/shard_map/dot_general | solution.py:117
  560.6 28.2 %all_to_all.10 = bf16[2,512,2048]{2,1,0:T(8,128)(2,1)S(1)} all-to-all(bf16[2,512,2048]{2,1,0:T(8,128)(2,1)} %bitcast.39), channel_id=1, replica_groups=mesh['rep'=2,'fs'=32,'tp'=2] {'tp'}, dimensions={0} | all-to-all | bytes 8388608 | tf_op jit(solution)/shard_map/all_to_all | solution.py:43
  591.0 2.1 add_convert_fusion
  (46 shorter events, 8.3 us)
Async XLA Ops:
  6.5 14.2 %copy-start.5 = (bf16[2048]{0:T(1024)(128)(2,1)S(1)}, bf16[2048]{0:T(1024)(128)(2,1)}, u32[]{:S(2)}) copy-start(bf16[2048]{0:T(1024)(128)(2,1)} %param.14) | copy-start | bytes 12292
  6.5 14.2 %copy-start.9 = (bf16[4,128]{1,0:T(4,128)(2,1)S(1)}, bf16[4,128]{1,0:T(4,128)(2,1)}, u32[]{:S(2)}) copy-start(bf16[4,128]{1,0:T(4,128)(2,1)} %param.18) | copy-start | bytes 3076
  6.5 14.2 %copy-start.8 = (bf16[1024]{0:T(1024)(128)(2,1)S(1)}, bf16[1024]{0:T(1024)(128)(2,1)}, u32[]{:S(2)}) copy-start(bf16[1024]{0:T(1024)(128)(2,1)} %param.19) | copy-start | bytes 6148
  6.5 14.2 %copy-start.7 = (bf16[1024]{0:T(1024)(128)(2,1)S(1)}, bf16[1024]{0:T(1024)(128)(2,1)}, u32[]{:S(2)}) copy-start(bf16[1024]{0:T(1024)(128)(2,1)} %param.20) | copy-start | bytes 6148
  6.5 150.5 %all-gather.7.cloned.1.call-start = ((), (), s32[]{:S(2)}) async-start(), calls=%async_computation.2 | async-start | bytes 4325376 | tf_op jit(solution)/shard_map/all_gather | solution.py:13
  8.2 309.6 %all-gather.13.cloned.1.call-start = ((), (), s32[]{:S(2)}) async-start(), calls=%async_computation.5 | async-start | bytes 5947392 | tf_op jit(solution)/shard_map/all_gather | solution.py:114
  11.3 179.8 %all-to-all-start = ((bf16[32,512,64]{1,2,0:T(8,128)(2,1)}), bf16[32,512,64]{1,2,0:T(8,128)(2,1)}, u32[]{:S(2)}, u32[]{:S(2)}) async-start(bf16[32,512,64]{1,2,0:T(8,128)(2,1)} %broadcast_in_dim.13), calls=%async_computation | async-start | bytes 4194304 | tf_op jit(solution)/shard_map/all_to_all | solution.py:18
  20.7 352.1 %all-gather.11.cloned.1.call-start = ((), (), s32[]{:S(2)}) async-start(), calls=%async_computation.4 | async-start | bytes 25165824 | tf_op jit(solution)/shard_map/all_gather | solution.py:33
  183.7 1.6 copy-start.1
  185.3 1.1 copy-start.4
  202.8 0.9 copy-start.2
  202.8 1.0 copy-start.3
  202.8 1.8 copy-start.6
  202.8 325.0 %all-gather.9.cloned.1.call-start = ((), (), s32[]{:S(2)}) async-start(), calls=%async_computation.3 | async-start | bytes 11894784 | tf_op jit(solution)/shard_map/all_gather | solution.py:13
  588.8 2.2 copy-start
Sparse Core Ops, SparseCore 0:
  9.0 147.9 all-gather.6
  158.7 159.0 all-gather.12
  319.4 53.3 all-gather.10
  374.2 153.5 all-gather.8
